TPU v7x, 32 devices: a whole 2x2x4 slice. The times are simulated.
32 devices in a mesh: sp: 8 (over z, y), tp: 4 (over x, core).
Axes of the slice: x: 2, y: 2, z: 4, core: 2. Of those that a mesh axis runs over, the one named last changes fastest.
Arguments:
- stream: bfloat16 [2048, 2048], P('sp', 'tp'), may hold values from -6 to 6
- norm_gain: float32 [2, 2048], replicated, may hold values from 0.1 to 1.9
- w_value: bfloat16 [2, 2048, 1024], P(None, 'sp', 'tp'), may hold values from -0.125 to 0.125
- w_gate: bfloat16 [2, 2048, 1024], P(None, 'sp', 'tp'), may hold values from -0.125 to 0.125
- conv_taps: float32 [2, 128, 1024], P(None, None, 'tp'), as said below
- channel_gain: float32 [2, 1024], P(None, 'tp'), may hold values from 0.1 to 1.9
- w_out: bfloat16 [2, 1024, 2048], P(None, 'tp', 'sp'), may hold values from -0.1875 to 0.1875
Outputs:
- result: bfloat16 [2048, 2048], P('sp', 'tp')
Inputs may be any that keep to these rules, and one draw needn't show every extreme that they name: `conv_taps`: taps of each block of 128 consecutive channels share a scale factor of its own.
All inputs are finite; a program needn't handle non-finite values.
Results may differ from a plain program's by a relative error of at most 0.012.
Values may be sent and summed in bfloat16 or wider, within the bound.
A program may use at most 64 MiB of HBM per device.

v0:
```python
import jax
import jax.numpy as jnp
from jax import lax
from jax.sharding import PartitionSpec as P

C = 1024
LAYERS = 2


def from_behind(value, axis, steps):
    count = lax.axis_size(axis)
    initial, last = (max(0, -steps), min(count, count - steps))
    return lax.ppermute(value, axis, [(source, source + steps) for source in range(initial, last)])


def shards(stream, norm_gain, w_value, w_gate, conv_taps, channel_gain, w_out):
    x = stream
    tokens_here = stream.shape[0]
    local_ch = w_value.shape[2]
    taps = conv_taps.shape[1]
    for layer in range(LAYERS):
        whole = lax.all_gather(x, "tp", axis=1, tiled=True).astype(jnp.float32)
        normed = (
            whole
            * lax.rsqrt(jnp.mean(whole * whole, axis=1, keepdims=True) + 1e-06)
            * norm_gain[layer]
        ).astype(jnp.bfloat16)
        value_whole, gate_whole = (
            lax.all_gather(w_value[layer], "sp", axis=0, tiled=True),
            lax.all_gather(w_gate[layer], "sp", axis=0, tiled=True),
        )
        value = jnp.dot(normed, value_whole, preferred_element_type=jnp.float32)
        gate = jnp.dot(normed, gate_whole, preferred_element_type=jnp.float32)
        glu = (value * jax.nn.sigmoid(gate)).astype(jnp.bfloat16)
        before = from_behind(glu[tokens_here - taps :], "sp", 1)
        padded = jnp.concatenate([before[1:], glu], axis=0).astype(jnp.float32)
        conv = lax.conv_general_dilated(
            padded[None],
            conv_taps[layer][:, None, :],
            (1,),
            "VALID",
            dimension_numbers=("NWC", "WIO", "NWC"),
            feature_group_count=local_ch,
            precision=lax.Precision.HIGHEST,
        )[0]
        mean = lax.psum(jnp.sum(conv, axis=1, keepdims=True), "tp") / C
        centred = conv - mean
        spread = lax.psum(jnp.sum(centred * centred, axis=1, keepdims=True), "tp") / C
        act = jax.nn.silu(centred * lax.rsqrt(spread + 1e-05) * channel_gain[layer]).astype(
            jnp.bfloat16
        )
        out_whole = lax.all_gather(w_out[layer], "sp", axis=1, tiled=True)
        terms = jnp.dot(act, out_whole, preferred_element_type=jnp.float32)
        branch = lax.psum_scatter(terms, "tp", scatter_dimension=1, tiled=True)
        x = (x.astype(jnp.float32) + branch).astype(jnp.bfloat16)
    return x


def solution(mesh):
    return jax.shard_map(
        shards,
        mesh=mesh,
        in_specs=(
            P("sp", "tp"),
            P(),
            P(None, "sp", "tp"),
            P(None, "sp", "tp"),
            P(None, None, "tp"),
            P(None, "tp"),
            P(None, "tp", "sp"),
        ),
        out_specs=P("sp", "tp"),
        check_vma=False,
    )
```

profile of v0, /device:TPU:0, one launch (start us, length us, event | category | flops | bytes accessed | tf_op | source)
XLA Modules:
  0.0 370.0 jit_solution(6867189528916284857)
XLA Ops:
  12.7 15.7 %all-gather.15.cloned.1.call-done = bf16[256,2048]{1,0:T(8,128)(2,1)} async-done(((bf16[256,512]{1,0:T(8,128)(2,1)}), bf16[256,2048]{1,0:T(8,128)(2,1)}) %all-gather.15.cloned.1.call-update) | async-done | bytes 1048592 | tf_op jit(solution)/shard_map/all_gather | solution.py:22
  30.0 40.8 %all-gather.19.cloned.1.call-done = bf16[1,2048,256]{2,1,0:T(8,128)(2,1)} async-done(((bf16[1,256,256]{2,1,0:T(8,128)(2,1)}), bf16[1,2048,256]{2,1,0:T(8,128)(2,1)}) %all-gather.19.cloned.1.call-update) | async-done | bytes 1048592 | tf_op jit(solution)/shard_map/all_gather | solution.py:29
  70.8 2.0 fusion.24
  72.8 39.1 %all-gather.21.cloned.1.call-done = bf16[1,2048,256]{2,1,0:T(8,128)(2,1)} async-done(((bf16[1,256,256]{2,1,0:T(8,128)(2,1)}), bf16[1,2048,256]{2,1,0:T(8,128)(2,1)}) %all-gather.21.cloned.1.call-update) | async-done | bytes 1048592 | tf_op jit(solution)/shard_map/all_gather | solution.py:30
  113.7 2.5 collective-permute-start
  116.2 1.9 collective-permute-done
  118.1 4.8 %fusion.50 = (f32[256]{0:T(256)S(1)}, f32[1,256,256]{2,0,1:T(1,128)S(1)}) fusion(f32[1,128,256]{2,1,0:T(8,128)S(1)} %get-tuple-element.6, bf16[1,383,256]{2,1,0:T(8,128)(2,1)S(1)} %maximum_bitcast_fusion), kind=kOutput, calls=%fused_computation.70 | convolution fusion | flops 100728576 | bytes 590336 | tf_op jit(solution)/shard_map/conv_general_dilated | solution.py:37
  123.0 5.7 %psum.28 = f32[256,1]{0,1:T(1,128)S(1)} all-reduce(f32[256,1]{0,1:T(1,128)S(1)} %bitcast.72), channel_id=1, replica_groups=mesh['sp'=8,'tp'=4] {'tp'}, use_global_device_ids=true, to_apply=%region_2.0 | all-reduce | flops 256 | bytes 2048 | tf_op jit(solution)/shard_map/psum | solution.py:46
  128.8 7.0 %psum.29 = f32[256,1]{0,1:T(1,128)S(1)} all-reduce(f32[256,1]{0,1:T(1,128)S(1)} %bitcast.68), channel_id=1, replica_groups=mesh['sp'=8,'tp'=4] {'tp'}, use_global_device_ids=true, to_apply=%region_4.0 | all-reduce | flops 256 | bytes 2048 | tf_op jit(solution)/shard_map/psum | solution.py:48
  135.8 16.2 %all-gather.23.cloned.1.call-done = bf16[1,256,2048]{2,1,0:T(8,128)(2,1)} async-done(((bf16[1,256,256]{2,1,0:T(8,128)(2,1)}), bf16[1,256,2048]{2,1,0:T(8,128)(2,1)}) %all-gather.23.cloned.1.call-update) | async-done | bytes 1048592 | tf_op jit(solution)/shard_map/all_gather | solution.py:52
  152.0 3.1 fusion.21
  155.2 30.3 %reduce-scatter.3.cloned.1.call-done = f32[256,512]{1,0:T(8,128)} async-done(((f32[256,2048]{1,0:T(8,128)}), f32[256,512]{1,0:T(8,128)}) %reduce-scatter.3.cloned.1.call-update) | async-done | bytes 524304 | tf_op jit(solution)/shard_map/reduce_scatter | solution.py:54
  189.6 14.6 %all-gather.17.cloned.1.call-done = bf16[256,2048]{1,0:T(8,128)(2,1)} async-done(((bf16[256,512]{1,0:T(8,128)(2,1)}), bf16[256,2048]{1,0:T(8,128)(2,1)}) %all-gather.17.cloned.1.call-update) | async-done | bytes 1048592 | tf_op jit(solution)/shard_map/all_gather | solution.py:22
  205.8 40.8 %all-gather.25.cloned.1.call-done = bf16[1,2048,256]{2,1,0:T(8,128)(2,1)} async-done(((bf16[1,256,256]{2,1,0:T(8,128)(2,1)}), bf16[1,2048,256]{2,1,0:T(8,128)(2,1)}) %all-gather.25.cloned.1.call-update) | async-done | bytes 1048592 | tf_op jit(solution)/shard_map/all_gather | solution.py:29
  246.6 2.0 fusion.19
  248.6 39.1 %all-gather.27.cloned.1.call-done = bf16[1,2048,256]{2,1,0:T(8,128)(2,1)} async-done(((bf16[1,256,256]{2,1,0:T(8,128)(2,1)}), bf16[1,2048,256]{2,1,0:T(8,128)(2,1)}) %all-gather.27.cloned.1.call-update) | async-done | bytes 1048592 | tf_op jit(solution)/shard_map/all_gather | solution.py:30
  289.5 2.5 collective-permute-start.1
  292.0 1.9 collective-permute-done.1
  293.9 4.8 %fusion.51 = (f32[256]{0:T(256)S(1)}, f32[1,256,256]{2,0,1:T(1,128)S(1)}) fusion(f32[1,128,256]{2,1,0:T(8,128)S(1)} %get-tuple-element.5, bf16[1,383,256]{2,1,0:T(8,128)(2,1)S(1)} %maximum_bitcast_fusion.1), kind=kOutput, calls=%fused_computation.71 | convolution fusion | flops 100728576 | bytes 590336 | tf_op jit(solution)/shard_map/conv_general_dilated | solution.py:37
  298.8 5.7 %psum.30 = f32[256,1]{0,1:T(1,128)S(1)} all-reduce(f32[256,1]{0,1:T(1,128)S(1)} %bitcast.73), channel_id=1, replica_groups=mesh['sp'=8,'tp'=4] {'tp'}, use_global_device_ids=true, to_apply=%region_8.9 | all-reduce | flops 256 | bytes 2048 | tf_op jit(solution)/shard_map/psum | solution.py:46
  304.6 7.0 %psum.31 = f32[256,1]{0,1:T(1,128)S(1)} all-reduce(f32[256,1]{0,1:T(1,128)S(1)} %bitcast.69), channel_id=1, replica_groups=mesh['sp'=8,'tp'=4] {'tp'}, use_global_device_ids=true, to_apply=%region_10.11 | all-reduce | flops 256 | bytes 2048 | tf_op jit(solution)/shard_map/psum | solution.py:48
  311.6 16.3 %all-gather.29.cloned.1.call-done = bf16[1,256,2048]{2,1,0:T(8,128)(2,1)} async-done(((bf16[1,256,256]{2,1,0:T(8,128)(2,1)}), bf16[1,256,2048]{2,1,0:T(8,128)(2,1)}) %all-gather.29.cloned.1.call-update) | async-done | bytes 1048592 | tf_op jit(solution)/shard_map/all_gather | solution.py:52
  327.9 3.1 fusion.16
  331.1 30.3 %reduce-scatter.5.cloned.1.call-done = f32[256,512]{1,0:T(8,128)} async-done(((f32[256,2048]{1,0:T(8,128)}), f32[256,512]{1,0:T(8,128)}) %reduce-scatter.5.cloned.1.call-update) | async-done | bytes 524304 | tf_op jit(solution)/shard_map/reduce_scatter | solution.py:54
  (60 shorter events, 19.2 us)
Async XLA Ops:
  6.5 6.1 %copy-start.5 = (f32[2,2048]{1,0:T(2,128)S(1)}, f32[2,2048]{1,0:T(2,128)}, u32[]{:S(2)}) copy-start(f32[2,2048]{1,0:T(2,128)} %param.8) | copy-start | bytes 49156
  6.5 6.1 %copy-start.4 = (f32[2,128,256]{2,1,0:T(8,128)S(1)}, f32[2,128,256]{2,1,0:T(8,128)}, u32[]{:S(2)}) copy-start(f32[2,128,256]{2,1,0:T(8,128)} %param.11) | copy-start | bytes 786436
  6.5 21.8 %all-gather.15.cloned.1.call-start = ((), (), s32[]{:S(2)}) async-start(), calls=%async_computation.2 | async-start | bytes 1310720 | tf_op jit(solution)/shard_map/all_gather | solution.py:22
  7.3 63.5 %all-gather.19.cloned.1.call-start = ((), (), s32[]{:S(2)}) async-start(), calls=%async_computation.6 | async-start | bytes 1179648 | tf_op jit(solution)/shard_map/all_gather | solution.py:29
  9.0 102.9 %all-gather.21.cloned.1.call-start = ((), (), s32[]{:S(2)}) async-start(), calls=%async_computation.7 | async-start | bytes 1179648 | tf_op jit(solution)/shard_map/all_gather | solution.py:30
  10.8 141.2 %all-gather.23.cloned.1.call-start = ((), (), s32[]{:S(2)}) async-start(), calls=%async_computation.8 | async-start | bytes 1179648 | tf_op jit(solution)/shard_map/all_gather | solution.py:52
  12.6 172.9 %reduce-scatter.3.cloned.1.call-start = ((), (), s32[]{:S(2)}) async-start(), calls=%async_computation.3 | async-start | bytes 2621440 | tf_op jit(solution)/shard_map/reduce_scatter | solution.py:54
  28.4 83.6 %copy-start.1 = (bf16[256,2048]{1,0:T(8,128)(2,1)S(1)}, bf16[256,2048]{1,0:T(8,128)(2,1)}, u32[]{:S(2)}) copy-start(bf16[256,2048]{1,0:T(8,128)(2,1)} %all-gather.15.cloned.1.call-done) | copy-start | bytes 3145732
  72.8 43.4 %copy-start.6 = (f32[2,256]{1,0:T(2,128)S(1)}, f32[2,256]{1,0:T(2,128)}, u32[]{:S(2)}) copy-start(f32[2,256]{1,0:T(2,128)} %param.12) | copy-start | bytes 6148
  113.7 4.4 %collective-permute-start = (bf16[128,256]{1,0:T(8,128)(2,1)S(1)}, bf16[128,256]{1,0:T(8,128)(2,1)S(1)}, u32[]{:S(2)}, u32[]{:S(2)}) collective-permute-start(bf16[128,256]{1,0:T(8,128)(2,1)S(1)} %slice.64), channel_id=1, source_target_pairs={{0,4},{4,8},{8,12},{12,16},{16,20},{20,24},{24,28},{1,5},{5,9},{9,... | collective-permute-start | bytes 196616 | tf_op jit(solution)/shard_map/ppermute | solution.py:13
  152.0 33.5 %copy-start.3 = (bf16[256,512]{1,0:T(8,128)(2,1)S(1)}, bf16[256,512]{1,0:T(8,128)(2,1)}, u32[]{:S(2)}) copy-start(bf16[256,512]{1,0:T(8,128)(2,1)} %param.7) | copy-start | bytes 786436
  155.1 49.0 %all-gather.17.cloned.1.call-start = ((), (), s32[]{:S(2)}) async-start(), calls=%async_computation.4 | async-start | bytes 1310720 | tf_op jit(solution)/shard_map/all_gather | solution.py:22
  187.3 59.3 %all-gather.25.cloned.1.call-start = ((), (), s32[]{:S(2)}) async-start(), calls=%async_computation.9 | async-start | bytes 1179648 | tf_op jit(solution)/shard_map/all_gather | solution.py:29
  188.0 99.7 %all-gather.27.cloned.1.call-start = ((), (), s32[]{:S(2)}) async-start(), calls=%async_computation.10 | async-start | bytes 1179648 | tf_op jit(solution)/shard_map/all_gather | solution.py:30
  188.8 139.1 %all-gather.29.cloned.1.call-start = ((), (), s32[]{:S(2)}) async-start(), calls=%async_computation.11 | async-start | bytes 1179648 | tf_op jit(solution)/shard_map/all_gather | solution.py:52
  189.5 171.9 %reduce-scatter.5.cloned.1.call-start = ((), (), s32[]{:S(2)}) async-start(), calls=%async_computation.5 | async-start | bytes 2621440 | tf_op jit(solution)/shard_map/reduce_scatter | solution.py:54
  204.1 83.6 %copy-start.2 = (bf16[256,2048]{1,0:T(8,128)(2,1)S(1)}, bf16[256,2048]{1,0:T(8,128)(2,1)}, u32[]{:S(2)}) copy-start(bf16[256,2048]{1,0:T(8,128)(2,1)} %all-gather.17.cloned.1.call-done) | copy-start | bytes 3145732
  289.5 4.4 %collective-permute-start.1 = (bf16[128,256]{1,0:T(8,128)(2,1)S(1)}, bf16[128,256]{1,0:T(8,128)(2,1)S(1)}, u32[]{:S(2)}, u32[]{:S(2)}) collective-permute-start(bf16[128,256]{1,0:T(8,128)(2,1)S(1)} %slice.66), channel_id=1, source_target_pairs={{0,4},{4,8},{8,12},{12,16},{16,20},{20,24},{24,28},{1,5},{5,9},{9,... | collective-permute-start | bytes 196616 | tf_op jit(solution)/shard_map/ppermute | solution.py:13
  327.9 33.5 %copy-start = (bf16[256,512]{1,0:T(8,128)(2,1)S(1)}, bf16[256,512]{1,0:T(8,128)(2,1)}, u32[]{:S(2)}) copy-start(bf16[256,512]{1,0:T(8,128)(2,1)} %add_convert_fusion.1) | copy-start | bytes 786436
Sparse Core Ops, SparseCore 0:
  8.9 19.4 all-gather.14
  30.5 40.2 all-gather.18
  72.9 38.9 all-gather.20
  113.8 38.0 all-gather.22
  155.2 30.1 reduce-scatter.2
  187.4 16.6 all-gather.16
  206.3 40.2 all-gather.24
  248.7 38.9 all-gather.26
  289.8 38.0 all-gather.28
  331.2 30.1 reduce-scatter.4
where the time goes:
time: 371 us; the launch traced here: 370 us
  waiting for transfers between devices  290 us (78%)
  blocking collectives  25.3 us (7%)
  matrix products  23.4 us (6%)
  between operations  13.7 us (4%)
  other arithmetic  7.31 us (2%)
  starting transfers between devices  5.32 us (1%)
  local copies, waits for them, and re-layouts  5.19 us (1%)
    all_gather x2, waiting for transfers between devices, shards(): lax.all_gather(w_value[layer], 'sp', axis=0, tiled=True)  81.7 us
    all_gather x2, waiting for transfers between devices, shards(): lax.all_gather(w_gate[layer], 'sp', axis=0, tiled=True)  78.2 us
    reduce_scatter x2, waiting for transfers between devices, shards(): branch = lax.psum_scatter(terms, 'tp', scatter_dimension=1, tiled=True)  60.6 us
    all_gather x2, waiting for transfers between devices, shards(): out_whole = lax.all_gather(w_out[layer], 'sp', axis=1, tiled=True)  32.5 us
    all_gather x2, waiting for transfers between devices, shards(): whole = lax.all_gather(x, 'tp', axis=1, tiled=True).astype(jnp.float32)  30.3 us
    psum x2, blocking collectives, shards(): lax.psum(jnp.sum(centred * centred, axis=1, keepdims=True), 'tp') / C  14 us
    psum x2, blocking collectives, shards(): mean = lax.psum(jnp.sum(conv, axis=1, keepdims=True), 'tp') / C  11.3 us
    conv_general_dilated x2, matrix products, shards(): lax.conv_general_dilated(padded[None], conv_taps[layer][:, None, :], (1,)...  9.67 us
  transfers between devices with their start and end apart: 12, of which 12 were waited for; matrix products, arithmetic and copies ran while one was open for 7% of the time, Pallas kernels for 0%

commit v1 on v0

--- a/solution.py
+++ b/solution.py
@@ -49,7 +49,14 @@
         act = jax.nn.silu(centred * lax.rsqrt(spread + 1e-05) * channel_gain[layer]).astype(
             jnp.bfloat16
         )
-        out_whole = lax.all_gather(w_out[layer], "sp", axis=1, tiled=True)
+        ring = [w_out[layer]]
+        for hop in range(7):
+            ring.append(lax.ppermute(ring[-1], "sp", [(dev, (dev + 1) % 8) for dev in range(8)]))
+        out_whole = jnp.roll(
+            jnp.concatenate(ring[::-1], axis=1),
+            (lax.axis_index("sp") + 1) * ring[0].shape[1],
+            axis=1,
+        )
         terms = jnp.dot(act, out_whole, preferred_element_type=jnp.float32)
         branch = lax.psum_scatter(terms, "tp", scatter_dimension=1, tiled=True)
         x = (x.astype(jnp.float32) + branch).astype(jnp.bfloat16)

time: 371 us -> 347 us (0.935)
  waiting for transfers between devices: 290 us -> 258 us
  local copies, waits for them, and re-layouts: 5.19 us -> 9.99 us
  starting transfers between devices: 5.32 us -> 9.83 us
    ppermute x0 -> x14, waiting for transfers between devices: none -> 64.5 us  [shards(): lax.ppermute(ring[-1], 'sp', [(dev, (dev + 1) % 8) for dev in range(8)])]
    all_gather x2, waiting for transfers between devices: 81.7 us -> 40.7 us  [shards(): lax.all_gather(w_value[layer], 'sp', axis=0, tiled=True)]
    all_gather x2 -> x0, waiting for transfers between devices: 32.5 us -> none  [shards(): out_whole = lax.all_gather(w_out[layer], 'sp', axis=1, tiled=True)]
    all_gather x2, waiting for transfers between devices: 30.3 us -> 15.5 us  [shards(): whole = lax.all_gather(x, 'tp', axis=1, tiled=True).astype(jnp.float32)]
    all_gather x2, waiting for transfers between devices: 78.2 us -> 68.2 us  [shards(): lax.all_gather(w_gate[layer], 'sp', axis=0, tiled=True)]
    unnamed x14 -> x30, local copies, waits for them, and re-layouts: 0.03 us -> 4.86 us
    ppermute x0 -> x14, starting transfers between devices: none -> 4.6 us  [shards(): lax.ppermute(ring[-1], 'sp', [(dev, (dev + 1) % 8) for dev in range(8)])]
  transfers between devices with their start and end apart: 12 -> 24, of which waited for: 12 -> 22; matrix products, arithmetic and copies ran while one was open for 7% -> 5% of each run, Pallas kernels for 0% -> 0%
where the time goes in v1:
time: 347 us; the launch traced here: 346 us
  waiting for transfers between devices  258 us (74%)
  blocking collectives  24.5 us (7%)
  matrix products  22.6 us (7%)
  between operations  13.7 us (4%)
  local copies, waits for them, and re-layouts  9.99 us (3%)
  starting transfers between devices  9.83 us (3%)
  other arithmetic  7.32 us (2%)
    all_gather x2, waiting for transfers between devices, shards(): lax.all_gather(w_gate[layer], 'sp', axis=0, tiled=True)  68.2 us
    ppermute x14, waiting for transfers between devices, shards(): lax.ppermute(ring[-1], 'sp', [(dev, (dev + 1) % 8) for dev in range(8)])  64.5 us
    reduce_scatter x2, waiting for transfers between devices, shards(): branch = lax.psum_scatter(terms, 'tp', scatter_dimension=1, tiled=True)  64.2 us
    all_gather x2, waiting for transfers between devices, shards(): lax.all_gather(w_value[layer], 'sp', axis=0, tiled=True)  40.7 us
    all_gather x2, waiting for transfers between devices, shards(): whole = lax.all_gather(x, 'tp', axis=1, tiled=True).astype(jnp.float32)  15.5 us
    psum x2, blocking collectives, shards(): lax.psum(jnp.sum(centred * centred, axis=1, keepdims=True), 'tp') / C  13.2 us
    psum x2, blocking collectives, shards(): mean = lax.psum(jnp.sum(conv, axis=1, keepdims=True), 'tp') / C  11.3 us
    conv_general_dilated x2, matrix products, shards(): lax.conv_general_dilated(padded[None], conv_taps[layer][:, None, :], (1,)...  9.67 us
  transfers between devices with their start and end apart: 24, of which 22 were waited for; matrix products, arithmetic and copies ran while one was open for 5% of the time, Pallas kernels for 0%

profile of v1, /device:TPU:0, one launch (start us, length us, event | category | flops | bytes accessed | tf_op | source)
XLA Modules:
  0.0 346.1 jit_solution(10852301936190354861)
XLA Ops:
  14.6 5.9 %collective-permute-done.9 = bf16[256,256]{1,0:T(8,128)(2,1)S(1)} collective-permute-done((bf16[256,256]{1,0:T(8,128)(2,1)S(1)}, bf16[256,256]{1,0:T(8,128)(2,1)S(1)}, u32[]{:S(2)}, u32[]{:S(2)}) %collective-permute-start.9) | collective-permute-done | bytes 131104 | tf_op jit(solution)/shard_map/ppermute | solution.py:54
  22.4 6.9 %collective-permute-done.10 = bf16[256,256]{1,0:T(8,128)(2,1)S(1)} collective-permute-done((bf16[256,256]{1,0:T(8,128)(2,1)S(1)}, bf16[256,256]{1,0:T(8,128)(2,1)S(1)}, u32[]{:S(2)}, u32[]{:S(2)}) %collective-permute-start.10) | collective-permute-done | bytes 131104 | tf_op jit(solution)/shard_map/ppermute | solution.py:54
  31.2 7.1 %collective-permute-done.11 = bf16[256,256]{1,0:T(8,128)(2,1)S(1)} collective-permute-done((bf16[256,256]{1,0:T(8,128)(2,1)S(1)}, bf16[256,256]{1,0:T(8,128)(2,1)S(1)}, u32[]{:S(2)}, u32[]{:S(2)}) %collective-permute-start.11) | collective-permute-done | bytes 131104 | tf_op jit(solution)/shard_map/ppermute | solution.py:54
  40.8 9.0 %collective-permute-done.12 = bf16[256,256]{1,0:T(8,128)(2,1)S(1)} collective-permute-done((bf16[256,256]{1,0:T(8,128)(2,1)S(1)}, bf16[256,256]{1,0:T(8,128)(2,1)S(1)}, u32[]{:S(2)}, u32[]{:S(2)}) %collective-permute-start.12) | collective-permute-done | bytes 131104 | tf_op jit(solution)/shard_map/ppermute | solution.py:54
  49.9 4.0 %collective-permute-done.4 = bf16[256,256]{1,0:T(8,128)(2,1)S(1)} collective-permute-done((bf16[256,256]{1,0:T(8,128)(2,1)S(1)}, bf16[256,256]{1,0:T(8,128)(2,1)S(1)}, u32[]{:S(2)}, u32[]{:S(2)}) %collective-permute-start.4) | collective-permute-done | bytes 131104 | tf_op jit(solution)/shard_map/ppermute | solution.py:54
  53.9 4.6 %collective-permute-done.13 = bf16[256,256]{1,0:T(8,128)(2,1)S(1)} collective-permute-done((bf16[256,256]{1,0:T(8,128)(2,1)S(1)}, bf16[256,256]{1,0:T(8,128)(2,1)S(1)}, u32[]{:S(2)}, u32[]{:S(2)}) %collective-permute-start.13) | collective-permute-done | bytes 131104 | tf_op jit(solution)/shard_map/ppermute | solution.py:54
  58.5 3.9 %collective-permute-done.5 = bf16[256,256]{1,0:T(8,128)(2,1)S(1)} collective-permute-done((bf16[256,256]{1,0:T(8,128)(2,1)S(1)}, bf16[256,256]{1,0:T(8,128)(2,1)S(1)}, u32[]{:S(2)}, u32[]{:S(2)}) %collective-permute-start.5) | collective-permute-done | bytes 131104 | tf_op jit(solution)/shard_map/ppermute | solution.py:54
  62.4 7.6 %collective-permute-done.14 = bf16[256,256]{1,0:T(8,128)(2,1)S(1)} collective-permute-done((bf16[256,256]{1,0:T(8,128)(2,1)S(1)}, bf16[256,256]{1,0:T(8,128)(2,1)S(1)}, u32[]{:S(2)}, u32[]{:S(2)}) %collective-permute-start.14) | collective-permute-done | bytes 131104 | tf_op jit(solution)/shard_map/ppermute | solution.py:54
  70.1 3.4 collective-permute-done.6
  73.5 4.3 %collective-permute-done.15 = bf16[256,256]{1,0:T(8,128)(2,1)S(1)} collective-permute-done((bf16[256,256]{1,0:T(8,128)(2,1)S(1)}, bf16[256,256]{1,0:T(8,128)(2,1)S(1)}, u32[]{:S(2)}, u32[]{:S(2)}) %collective-permute-start.15) | collective-permute-done | bytes 131104 | tf_op jit(solution)/shard_map/ppermute | solution.py:54
  78.0 3.2 collective-permute-done.7
  89.7 29.1 %all-gather.17.cloned.1.call-done = bf16[1,2048,256]{2,1,0:T(8,128)(2,1)} async-done(((bf16[1,256,256]{2,1,0:T(8,128)(2,1)}), bf16[1,2048,256]{2,1,0:T(8,128)(2,1)}) %all-gather.17.cloned.1.call-update) | async-done | bytes 1048592 | tf_op jit(solution)/shard_map/all_gather | solution.py:30
  124.9 4.8 %fusion.55 = (f32[256]{0:T(256)S(1)}, f32[1,256,256]{2,0,1:T(1,128)S(1)}) fusion(f32[1,128,256]{2,1,0:T(8,128)S(1)} %get-tuple-element.7, bf16[1,383,256]{2,1,0:T(8,128)(2,1)S(1)} %maximum_bitcast_fusion), kind=kOutput, calls=%fused_computation.95 | convolution fusion | flops 100728576 | bytes 590336 | tf_op jit(solution)/shard_map/conv_general_dilated | solution.py:37
  129.7 5.7 %psum.28 = f32[256,1]{0,1:T(1,128)S(1)} all-reduce(f32[256,1]{0,1:T(1,128)S(1)} %bitcast.72), channel_id=1, replica_groups=mesh['sp'=8,'tp'=4] {'tp'}, use_global_device_ids=true, to_apply=%region_2.0 | all-reduce | flops 256 | bytes 2048 | tf_op jit(solution)/shard_map/psum | solution.py:46
  135.6 6.6 %psum.29 = f32[256,1]{0,1:T(1,128)S(1)} all-reduce(f32[256,1]{0,1:T(1,128)S(1)} %bitcast.68), channel_id=1, replica_groups=mesh['sp'=8,'tp'=4] {'tp'}, use_global_device_ids=true, to_apply=%region_4.0 | all-reduce | flops 256 | bytes 2048 | tf_op jit(solution)/shard_map/psum | solution.py:48
  142.2 3.3 fusion.20
  145.6 32.0 %reduce-scatter.3.cloned.1.call-done = f32[256,512]{1,0:T(8,128)} async-done(((f32[256,2048]{1,0:T(8,128)}), f32[256,512]{1,0:T(8,128)}) %reduce-scatter.3.cloned.1.call-update) | async-done | bytes 524304 | tf_op jit(solution)/shard_map/reduce_scatter | solution.py:61
  180.8 15.5 %all-gather.13.cloned.1.call-done = bf16[256,2048]{1,0:T(8,128)(2,1)} async-done(((bf16[256,512]{1,0:T(8,128)(2,1)}), bf16[256,2048]{1,0:T(8,128)(2,1)}) %all-gather.13.cloned.1.call-update) | async-done | bytes 1048592 | tf_op jit(solution)/shard_map/all_gather | solution.py:22
  197.9 40.7 %all-gather.19.cloned.1.call-done = bf16[1,2048,256]{2,1,0:T(8,128)(2,1)} async-done(((bf16[1,256,256]{2,1,0:T(8,128)(2,1)}), bf16[1,2048,256]{2,1,0:T(8,128)(2,1)}) %all-gather.19.cloned.1.call-update) | async-done | bytes 1048592 | tf_op jit(solution)/shard_map/all_gather | solution.py:29
  240.6 39.1 %all-gather.21.cloned.1.call-done = bf16[1,2048,256]{2,1,0:T(8,128)(2,1)} async-done(((bf16[1,256,256]{2,1,0:T(8,128)(2,1)}), bf16[1,2048,256]{2,1,0:T(8,128)(2,1)}) %all-gather.21.cloned.1.call-update) | async-done | bytes 1048592 | tf_op jit(solution)/shard_map/all_gather | solution.py:30
  285.9 4.8 %fusion.56 = (f32[256]{0:T(256)S(1)}, f32[1,256,256]{2,0,1:T(1,128)S(1)}) fusion(f32[1,128,256]{2,1,0:T(8,128)S(1)} %get-tuple-element.6, bf16[1,383,256]{2,1,0:T(8,128)(2,1)S(1)} %maximum_bitcast_fusion.1), kind=kOutput, calls=%fused_computation.96 | convolution fusion | flops 100728576 | bytes 590336 | tf_op jit(solution)/shard_map/conv_general_dilated | solution.py:37
  290.7 5.7 %psum.30 = f32[256,1]{0,1:T(1,128)S(1)} all-reduce(f32[256,1]{0,1:T(1,128)S(1)} %bitcast.73), channel_id=1, replica_groups=mesh['sp'=8,'tp'=4] {'tp'}, use_global_device_ids=true, to_apply=%region_8.10 | all-reduce | flops 256 | bytes 2048 | tf_op jit(solution)/shard_map/psum | solution.py:46
  296.6 6.6 %psum.31 = f32[256,1]{0,1:T(1,128)S(1)} all-reduce(f32[256,1]{0,1:T(1,128)S(1)} %bitcast.69), channel_id=1, replica_groups=mesh['sp'=8,'tp'=4] {'tp'}, use_global_device_ids=true, to_apply=%region_10.12 | all-reduce | flops 256 | bytes 2048 | tf_op jit(solution)/shard_map/psum | solution.py:48
  305.3 32.1 %reduce-scatter.5.cloned.1.call-done = f32[256,512]{1,0:T(8,128)} async-done(((f32[256,2048]{1,0:T(8,128)}), f32[256,512]{1,0:T(8,128)}) %reduce-scatter.5.cloned.1.call-update) | async-done | bytes 524304 | tf_op jit(solution)/shard_map/reduce_scatter | solution.py:61
  (99 shorter events, 46.4 us)
Async XLA Ops:
  6.5 79.4 %all-gather.11.cloned.1.call-start = ((), (), s32[]{:S(2)}) async-start(), calls=%async_computation.2 | async-start | bytes 1310720 | tf_op jit(solution)/shard_map/all_gather | solution.py:22
  7.3 80.3 %all-gather.15.cloned.1.call-start = ((), (), s32[]{:S(2)}) async-start(), calls=%async_computation.6 | async-start | bytes 1179648 | tf_op jit(solution)/shard_map/all_gather | solution.py:29
  9.0 109.7 %all-gather.17.cloned.1.call-start = ((), (), s32[]{:S(2)}) async-start(), calls=%async_computation.7 | async-start | bytes 1179648 | tf_op jit(solution)/shard_map/all_gather | solution.py:30
  10.1 10.4 %collective-permute-start.9 = (bf16[256,256]{1,0:T(8,128)(2,1)S(1)}, bf16[256,256]{1,0:T(8,128)(2,1)S(1)}, u32[]{:S(2)}, u32[]{:S(2)}) collective-permute-start(bf16[256,256]{1,0:T(8,128)(2,1)S(1)} %get-tuple-element.15), channel_id=1, source_target_pairs={{0,4},{4,8},{8,12},{12,16},{16,20},{20,24},{24,28},{28,0},{1,5},{5... | collective-permute-start | bytes 393224 | tf_op jit(solution)/shard_map/ppermute | solution.py:54
  13.1 9.3 %collective-permute-start.1 = (bf16[256,256]{1,0:T(8,128)(2,1)S(1)}, bf16[256,256]{1,0:T(8,128)(2,1)S(1)}, u32[]{:S(2)}, u32[]{:S(2)}) collective-permute-start(bf16[256,256]{1,0:T(8,128)(2,1)S(1)} %get-tuple-element.14), channel_id=1, source_target_pairs={{0,4},{4,8},{8,12},{12,16},{16,20},{20,24},{24,28},{28,0},{1,5},{5... | collective-permute-start | bytes 393224 | tf_op jit(solution)/shard_map/ppermute | solution.py:54
  20.5 8.8 %collective-permute-start.10 = (bf16[256,256]{1,0:T(8,128)(2,1)S(1)}, bf16[256,256]{1,0:T(8,128)(2,1)S(1)}, u32[]{:S(2)}, u32[]{:S(2)}) collective-permute-start(bf16[256,256]{1,0:T(8,128)(2,1)S(1)} %collective-permute-done.9), channel_id=1, source_target_pairs={{0,4},{4,8},{8,12},{12,16},{16,20},{20,24},{24,28},{28,0},{1,5},{5... | collective-permute-start | bytes 393224 | tf_op jit(solution)/shard_map/ppermute | solution.py:54
  22.4 8.8 %collective-permute-start.2 = (bf16[256,256]{1,0:T(8,128)(2,1)S(1)}, bf16[256,256]{1,0:T(8,128)(2,1)S(1)}, u32[]{:S(2)}, u32[]{:S(2)}) collective-permute-start(bf16[256,256]{1,0:T(8,128)(2,1)S(1)} %collective-permute-done.1), channel_id=1, source_target_pairs={{0,4},{4,8},{8,12},{12,16},{16,20},{20,24},{24,28},{28,0},{1,5},{5... | collective-permute-start | bytes 393224 | tf_op jit(solution)/shard_map/ppermute | solution.py:54
  29.3 9.1 %collective-permute-start.11 = (bf16[256,256]{1,0:T(8,128)(2,1)S(1)}, bf16[256,256]{1,0:T(8,128)(2,1)S(1)}, u32[]{:S(2)}, u32[]{:S(2)}) collective-permute-start(bf16[256,256]{1,0:T(8,128)(2,1)S(1)} %collective-permute-done.10), channel_id=1, source_target_pairs={{0,4},{4,8},{8,12},{12,16},{16,20},{20,24},{24,28},{28,0},{1,5},{5... | collective-permute-start | bytes 393224 | tf_op jit(solution)/shard_map/ppermute | solution.py:54
  31.2 9.6 %collective-permute-start.3 = (bf16[256,256]{1,0:T(8,128)(2,1)S(1)}, bf16[256,256]{1,0:T(8,128)(2,1)S(1)}, u32[]{:S(2)}, u32[]{:S(2)}) collective-permute-start(bf16[256,256]{1,0:T(8,128)(2,1)S(1)} %collective-permute-done.2), channel_id=1, source_target_pairs={{0,4},{4,8},{8,12},{12,16},{16,20},{20,24},{24,28},{28,0},{1,5},{5... | collective-permute-start | bytes 393224 | tf_op jit(solution)/shard_map/ppermute | solution.py:54
  38.4 11.5 %collective-permute-start.12 = (bf16[256,256]{1,0:T(8,128)(2,1)S(1)}, bf16[256,256]{1,0:T(8,128)(2,1)S(1)}, u32[]{:S(2)}, u32[]{:S(2)}) collective-permute-start(bf16[256,256]{1,0:T(8,128)(2,1)S(1)} %collective-permute-done.11), channel_id=1, source_target_pairs={{0,4},{4,8},{8,12},{12,16},{16,20},{20,24},{24,28},{28,0},{1,5},{5... | collective-permute-start | bytes 393224 | tf_op jit(solution)/shard_map/ppermute | solution.py:54
  40.1 137.5 %reduce-scatter.3.cloned.1.call-start = ((), (), s32[]{:S(2)}) async-start(), calls=%async_computation.3 | async-start | bytes 2621440 | tf_op jit(solution)/shard_map/reduce_scatter | solution.py:61
  40.8 13.1 %collective-permute-start.4 = (bf16[256,256]{1,0:T(8,128)(2,1)S(1)}, bf16[256,256]{1,0:T(8,128)(2,1)S(1)}, u32[]{:S(2)}, u32[]{:S(2)}) collective-permute-start(bf16[256,256]{1,0:T(8,128)(2,1)S(1)} %collective-permute-done.3), channel_id=1, source_target_pairs={{0,4},{4,8},{8,12},{12,16},{16,20},{20,24},{24,28},{28,0},{1,5},{5... | collective-permute-start | bytes 393224 | tf_op jit(solution)/shard_map/ppermute | solution.py:54
  49.9 8.6 %collective-permute-start.13 = (bf16[256,256]{1,0:T(8,128)(2,1)S(1)}, bf16[256,256]{1,0:T(8,128)(2,1)S(1)}, u32[]{:S(2)}, u32[]{:S(2)}) collective-permute-start(bf16[256,256]{1,0:T(8,128)(2,1)S(1)} %collective-permute-done.12), channel_id=1, source_target_pairs={{0,4},{4,8},{8,12},{12,16},{16,20},{20,24},{24,28},{28,0},{1,5},{5... | collective-permute-start | bytes 393224 | tf_op jit(solution)/shard_map/ppermute | solution.py:54
  53.9 8.6 %collective-permute-start.5 = (bf16[256,256]{1,0:T(8,128)(2,1)S(1)}, bf16[256,256]{1,0:T(8,128)(2,1)S(1)}, u32[]{:S(2)}, u32[]{:S(2)}) collective-permute-start(bf16[256,256]{1,0:T(8,128)(2,1)S(1)} %collective-permute-done.4), channel_id=1, source_target_pairs={{0,4},{4,8},{8,12},{12,16},{16,20},{20,24},{24,28},{28,0},{1,5},{5... | collective-permute-start | bytes 393224 | tf_op jit(solution)/shard_map/ppermute | solution.py:54
  58.5 11.6 %collective-permute-start.14 = (bf16[256,256]{1,0:T(8,128)(2,1)S(1)}, bf16[256,256]{1,0:T(8,128)(2,1)S(1)}, u32[]{:S(2)}, u32[]{:S(2)}) collective-permute-start(bf16[256,256]{1,0:T(8,128)(2,1)S(1)} %collective-permute-done.13), channel_id=1, source_target_pairs={{0,4},{4,8},{8,12},{12,16},{16,20},{20,24},{24,28},{28,0},{1,5},{5... | collective-permute-start | bytes 393224 | tf_op jit(solution)/shard_map/ppermute | solution.py:54
  62.4 11.1 %collective-permute-start.6 = (bf16[256,256]{1,0:T(8,128)(2,1)S(1)}, bf16[256,256]{1,0:T(8,128)(2,1)S(1)}, u32[]{:S(2)}, u32[]{:S(2)}) collective-permute-start(bf16[256,256]{1,0:T(8,128)(2,1)S(1)} %collective-permute-done.5), channel_id=1, source_target_pairs={{0,4},{4,8},{8,12},{12,16},{16,20},{20,24},{24,28},{28,0},{1,5},{5... | collective-permute-start | bytes 393224 | tf_op jit(solution)/shard_map/ppermute | solution.py:54
  70.1 7.8 %collective-permute-start.15 = (bf16[256,256]{1,0:T(8,128)(2,1)S(1)}, bf16[256,256]{1,0:T(8,128)(2,1)S(1)}, u32[]{:S(2)}, u32[]{:S(2)}) collective-permute-start(bf16[256,256]{1,0:T(8,128)(2,1)S(1)} %collective-permute-done.14), channel_id=1, source_target_pairs={{0,4},{4,8},{8,12},{12,16},{16,20},{20,24},{24,28},{28,0},{1,5},{5... | collective-permute-start | bytes 393224 | tf_op jit(solution)/shard_map/ppermute | solution.py:54
  73.5 7.7 %collective-permute-start.7 = (bf16[256,256]{1,0:T(8,128)(2,1)S(1)}, bf16[256,256]{1,0:T(8,128)(2,1)S(1)}, u32[]{:S(2)}, u32[]{:S(2)}) collective-permute-start(bf16[256,256]{1,0:T(8,128)(2,1)S(1)} %collective-permute-done.6), channel_id=1, source_target_pairs={{0,4},{4,8},{8,12},{12,16},{16,20},{20,24},{24,28},{28,0},{1,5},{5... | collective-permute-start | bytes 393224 | tf_op jit(solution)/shard_map/ppermute | solution.py:54
  120.5 4.4 %collective-permute-start = (bf16[128,256]{1,0:T(8,128)(2,1)S(1)}, bf16[128,256]{1,0:T(8,128)(2,1)S(1)}, u32[]{:S(2)}, u32[]{:S(2)}) collective-permute-start(bf16[128,256]{1,0:T(8,128)(2,1)S(1)} %slice.64), channel_id=1, source_target_pairs={{0,4},{4,8},{8,12},{12,16},{16,20},{20,24},{24,28},{1,5},{5,9},{9,... | collective-permute-start | bytes 196616 | tf_op jit(solution)/shard_map/ppermute | solution.py:13
  145.5 50.8 %all-gather.13.cloned.1.call-start = ((), (), s32[]{:S(2)}) async-start(), calls=%async_computation.4 | async-start | bytes 1310720 | tf_op jit(solution)/shard_map/all_gather | solution.py:22
  179.4 59.1 %all-gather.19.cloned.1.call-start = ((), (), s32[]{:S(2)}) async-start(), calls=%async_computation.8 | async-start | bytes 1179648 | tf_op jit(solution)/shard_map/all_gather | solution.py:29
  180.0 99.7 %all-gather.21.cloned.1.call-start = ((), (), s32[]{:S(2)}) async-start(), calls=%async_computation.9 | async-start | bytes 1179648 | tf_op jit(solution)/shard_map/all_gather | solution.py:30
  180.8 156.7 %reduce-scatter.5.cloned.1.call-start = ((), (), s32[]{:S(2)}) async-start(), calls=%async_computation.5 | async-start | bytes 2621440 | tf_op jit(solution)/shard_map/reduce_scatter | solution.py:61
  281.5 4.4 %collective-permute-start.8 = (bf16[128,256]{1,0:T(8,128)(2,1)S(1)}, bf16[128,256]{1,0:T(8,128)(2,1)S(1)}, u32[]{:S(2)}, u32[]{:S(2)}) collective-permute-start(bf16[128,256]{1,0:T(8,128)(2,1)S(1)} %slice.66), channel_id=1, source_target_pairs={{0,4},{4,8},{8,12},{12,16},{16,20},{20,24},{24,28},{1,5},{5,9},{9,... | collective-permute-start | bytes 196616 | tf_op jit(solution)/shard_map/ppermute | solution.py:13
  (8 other events, 372.6 us)
Sparse Core Ops, SparseCore 0:
  8.9 19.4 all-gather.10
  30.5 46.4 all-gather.14
  79.1 39.5 all-gather.16
  145.6 31.9 reduce-scatter.2
  179.6 16.6 all-gather.12
  198.3 40.2 all-gather.18
  240.7 38.9 all-gather.20
  305.4 31.9 reduce-scatter.4
